TPU v7x, 32 devices: a whole 2x2x4 slice. The times are simulated.
32 devices in a mesh: ep: 8 (over z, y), tp: 4 (over x, core).
Axes of the slice: x: 2, y: 2, z: 4, core: 2. Of those that a mesh axis runs over, the one named last changes fastest.
Arguments:
- tokens: bfloat16 [384, 2048], P(('ep', 'tp')), may hold values from -6 to 6
- cache_latent: bfloat16 [384, 1024, 512], P(('ep', 'tp')), may hold values from -1700 to 1700
- cache_rope: bfloat16 [384, 64, 1024], P(('ep', 'tp')), may hold values from -6 to 6
- lengths: int32 [384], P(('ep', 'tp')), may hold values from 128 to 1023, as said below
- attn_gain: bfloat16 [2048], replicated, may hold values from 0.099609375 to 1.8984375
- latent_gain: bfloat16 [512], replicated, may hold values from 0.099609375 to 1.8984375
- post_attn_gain: bfloat16 [2048], replicated, may hold values from 0.099609375 to 1.8984375
- ffn_gain: bfloat16 [2048], replicated, may hold values from 0.099609375 to 1.8984375
- post_ffn_gain: bfloat16 [2048], replicated, may hold values from 0.099609375 to 1.8984375
- w_query: bfloat16 [2048, 2048], P(None, 'tp'), may hold values from -0.125 to 0.125
- w_query_rot: bfloat16 [2048, 1024], P(None, 'tp'), may hold values from -0.125 to 0.125
- w_latent: bfloat16 [2048, 512], P(None, 'tp'), may hold values from -0.125 to 0.125
- w_key_rot: bfloat16 [2048, 64], replicated, may hold values from -0.125 to 0.125
- w_key_up: bfloat16 [512, 16, 128], P(None, 'tp'), may hold values from -0.25 to 0.25
- w_value_up: bfloat16 [512, 16, 128], P(None, 'tp'), may hold values from -0.25 to 0.25
- w_out: bfloat16 [2048, 2048], P('tp'), may hold values from -0.125 to 0.125
- route_logits: float32 [384, 4], P('ep'), may hold values from -6 to 6
- routes: int32 [384, 4], P('ep'), may hold values from 0 to 7, all different within a row; in each aligned block of 48 rows (0 to 47, 48 to 95, ...) at most 25 rows name the same one
- w_gate: bfloat16 [8, 2048, 2048], P('ep', None, 'tp'), may hold values from -0.3125 to 0.3125
- w_up: bfloat16 [8, 2048, 2048], P('ep', None, 'tp'), may hold values from -0.3125 to 0.3125
- w_down: bfloat16 [8, 2048, 2048], P('ep', 'tp'), may hold values from -0.125 to 0.125
Outputs:
- result: bfloat16 [384, 2048], P(('ep', 'tp'))
- new_latent: bfloat16 [384, 512], P(('ep', 'tp'))
- new_rope: bfloat16 [384, 64], P(('ep', 'tp'))
Inputs may be any that keep to these rules, and one draw needn't show every extreme that they name: Each sequence's cache holds positions 0 to lengths - 1, and the new token stands at position lengths; some sequence has 1023 in every draw. `routes`: each row names 4 different experts; in each aligned block of 48 rows (the tokens of one index of ep) no expert is named more than 25 times, a bound that some block reaches.
All inputs are finite; a program needn't handle non-finite values.
Results may differ from a plain program's by a relative error of at most 0.019.
Values may be sent and summed in bfloat16 or wider, within the bound.
A program may use at most 128 MiB of HBM per device.

v0:
```python
import jax
import jax.numpy as jnp
from jax import lax
from jax.sharding import PartitionSpec as P

eps_norm = 1e-06
clamp_limit = 7.0
sigmoid_alpha = 1.702
theta_base = 10000.0


def rms_scale(values, gain):
    mean_square = jnp.mean(values * values, axis=-1, keepdims=True)
    return values * lax.rsqrt(mean_square + eps_norm) * gain.astype(jnp.float32)


def rotate(values, positions):
    half = values.shape[-1] // 2
    freqs = theta_base ** (-jnp.arange(half, dtype=jnp.float32) / half)
    angles = positions[..., None] * freqs
    cosine = jnp.cos(angles)
    sine = jnp.sin(angles)
    first = values[..., :half]
    second = values[..., half:]
    return jnp.concatenate(
        [first * cosine - second * sine, second * cosine + first * sine], axis=-1
    )


def attend(
    query_latent, query_turned, cache_latent, cache_rope, new_latent, new_rope, lengths, scale
):
    sequences, heads, latent_size = query_latent.shape
    span = cache_latent.shape[1]
    stride = min(512, span)
    blocks_used = (jnp.max(lengths) + stride - 1) // stride

    def score_block(index, scores):
        offset = index * stride
        latents = lax.dynamic_slice_in_dim(cache_latent, offset, stride, 1)
        rotary = lax.dynamic_slice_in_dim(cache_rope, offset, stride, 2)
        block_scores = jnp.einsum(
            "shc,spc->shp", query_latent, latents, preferred_element_type=jnp.float32
        )
        block_scores = block_scores + jnp.einsum(
            "shr,srp->shp", query_turned, rotary, preferred_element_type=jnp.float32
        )
        return lax.dynamic_update_slice_in_dim(scores, block_scores * scale, offset, 2)

    scores = lax.fori_loop(
        0, blocks_used, score_block, jnp.zeros((sequences, heads, span), jnp.float32)
    )
    self_score = (
        jnp.einsum("shc,sc->sh", query_latent, new_latent, preferred_element_type=jnp.float32)
        + jnp.einsum("shr,sr->sh", query_turned, new_rope, preferred_element_type=jnp.float32)
    ) * scale
    valid = jnp.arange(span, dtype=jnp.int32)[None, None, :] < lengths[:, None, None]
    masked = jnp.where(valid, scores, -jnp.inf)
    highest = jnp.maximum(jnp.max(masked, axis=-1), self_score)
    raised = jnp.exp(masked - highest[..., None])
    raised_self = jnp.exp(self_score - highest)
    total = jnp.sum(raised, axis=-1) + raised_self
    probs = (raised / total[..., None]).astype(jnp.bfloat16)
    prob_self = (raised_self / total).astype(jnp.bfloat16)

    def read_block(index, summed):
        offset = index * stride
        latents = lax.dynamic_slice_in_dim(cache_latent, offset, stride, 1)
        weights = lax.dynamic_slice_in_dim(probs, offset, stride, 2)
        return summed + jnp.einsum(
            "shp,spc->shc", weights, latents, preferred_element_type=jnp.float32
        )

    summed = lax.fori_loop(
        0, blocks_used, read_block, jnp.zeros((sequences, heads, latent_size), jnp.float32)
    )
    summed = (
        summed
        + prob_self.astype(jnp.float32)[..., None] * new_latent.astype(jnp.float32)[:, None, :]
    )
    return summed.astype(jnp.bfloat16)


def body(
    tokens,
    cache_latent,
    cache_rope,
    lengths,
    attn_gain,
    latent_gain,
    post_attn_gain,
    ffn_gain,
    post_ffn_gain,
    w_query,
    w_query_rot,
    w_latent,
    w_key_rot,
    w_key_up,
    w_value_up,
    w_out,
    route_logits,
    routes,
    w_gate,
    w_up,
    w_down,
):
    own_rows, width = tokens.shape
    tensor_ways = lax.axis_size("tp")
    expert_ways = lax.axis_size("ep")
    latent_size, local_heads, key_size = w_key_up.shape
    rot_size = w_key_rot.shape[1]
    value_size = w_value_up.shape[2]
    group = own_rows * tensor_ways
    scale = (key_size + rot_size) ** (-0.5)
    token_values = tokens.astype(jnp.float32)
    normed = rms_scale(token_values, attn_gain).astype(jnp.bfloat16)
    key_raw = jnp.dot(normed, w_key_rot, preferred_element_type=jnp.float32).astype(jnp.bfloat16)
    group_rows = lax.all_gather(normed, "tp", axis=0, tiled=True)
    stacked = jnp.concatenate([w_query, w_query_rot, w_latent], axis=1)
    projected = jnp.dot(group_rows, stacked, preferred_element_type=jnp.float32).astype(
        jnp.bfloat16
    )
    plain_cols = local_heads * key_size
    rotary_cols = local_heads * rot_size
    query_plain = projected[:, :plain_cols].reshape(group, local_heads, key_size)
    query_rotary = projected[:, plain_cols : plain_cols + rotary_cols].reshape(
        group, local_heads, rot_size
    )
    latent_part = projected[:, plain_cols + rotary_cols :]
    query_latent = jnp.einsum(
        "ghn,chn->ghc", query_plain, w_key_up, preferred_element_type=jnp.float32
    ).astype(jnp.bfloat16)
    query_latent, query_rotary, latent_raw = (
        lax.all_to_all(query_latent, "tp", split_axis=0, concat_axis=1, tiled=True),
        lax.all_to_all(query_rotary, "tp", split_axis=0, concat_axis=1, tiled=True),
        lax.all_to_all(latent_part, "tp", split_axis=0, concat_axis=1, tiled=True),
    )
    positions = lengths.astype(jnp.float32)
    new_latent = rms_scale(latent_raw.astype(jnp.float32), latent_gain).astype(jnp.bfloat16)
    new_rope = rotate(key_raw.astype(jnp.float32), positions).astype(jnp.bfloat16)
    query_turned = rotate(query_rotary.astype(jnp.float32), positions[:, None]).astype(jnp.bfloat16)
    head_latent = attend(
        query_latent, query_turned, cache_latent, cache_rope, new_latent, new_rope, lengths, scale
    )
    head_latent = lax.all_to_all(head_latent, "tp", split_axis=1, concat_axis=0, tiled=True)
    values = jnp.einsum("ghc,chv->ghv", head_latent, w_value_up, preferred_element_type=jnp.float32)
    values = values.astype(jnp.bfloat16).reshape(group, local_heads * value_size)
    attn = lax.psum_scatter(
        jnp.dot(values, w_out, preferred_element_type=jnp.float32).astype(jnp.bfloat16),
        "tp",
        scatter_dimension=0,
        tiled=True,
    )
    mixed = (token_values + rms_scale(attn.astype(jnp.float32), post_attn_gain)).astype(
        jnp.bfloat16
    )
    ffn_input = rms_scale(mixed.astype(jnp.float32), ffn_gain).astype(jnp.bfloat16)
    group_inputs = lax.all_gather(ffn_input, "tp", axis=0, tiled=True)
    top_k = routes.shape[1]
    capacity = (group * top_k + expert_ways - 1) // expert_ways + 1
    flat_routes = routes.reshape(-1)
    onehot = (flat_routes[:, None] == jnp.arange(expert_ways, dtype=jnp.int32)[None, :]).astype(
        jnp.int32
    )
    rank = jnp.sum((jnp.cumsum(onehot, axis=0) - onehot) * onehot, axis=1)
    slot_of = (flat_routes * capacity + rank).reshape(group, top_k)
    slot_ids = jnp.arange(expert_ways * capacity, dtype=jnp.int32)
    hits = slot_of[:, :, None] == slot_ids[None, None, :]
    dispatch_map = jnp.any(hits, axis=1).astype(jnp.bfloat16)
    slots = jnp.einsum("gs,gd->sd", dispatch_map, group_inputs, preferred_element_type=jnp.float32)
    slots = slots.astype(jnp.bfloat16).reshape(expert_ways, capacity, width)
    gate_local = w_gate[0]
    up_local = w_up[0]
    down_local = w_down[0]
    column_block = width // tensor_ways
    sent = lax.dynamic_slice_in_dim(slots, lax.axis_index("tp") * column_block, column_block, 2)
    full_rows = lax.all_gather(
        lax.all_to_all(sent, "ep", split_axis=0, concat_axis=0, tiled=True),
        "tp",
        axis=2,
        tiled=True,
    )
    sources, count, _ = full_rows.shape
    flat = full_rows.reshape(sources * count, width)
    gate = jnp.minimum(jnp.dot(flat, gate_local, preferred_element_type=jnp.float32), clamp_limit)
    upward = jnp.clip(
        jnp.dot(flat, up_local, preferred_element_type=jnp.float32), -clamp_limit, clamp_limit
    )
    active = ((upward + 1.0) * gate * jax.nn.sigmoid(sigmoid_alpha * gate)).astype(jnp.bfloat16)
    partial_out = jnp.dot(active, down_local, preferred_element_type=jnp.float32)
    partial_out = partial_out.reshape(sources, count, width)
    summed = lax.psum_scatter(
        partial_out.astype(jnp.bfloat16), "tp", scatter_dimension=2, tiled=True
    )
    returned = lax.all_to_all(summed, "ep", split_axis=0, concat_axis=0, tiled=True)
    route_weights = jax.nn.softmax(route_logits, axis=-1)
    combine = jnp.sum(jnp.where(hits, route_weights[:, :, None], 0.0), axis=1)
    moe_part = jnp.dot(
        combine,
        returned.reshape(-1, returned.shape[2]).astype(jnp.float32),
        precision=lax.Precision.HIGHEST,
    ).astype(jnp.bfloat16)
    moe = lax.all_to_all(moe_part, "tp", split_axis=0, concat_axis=1, tiled=True)
    result = (mixed.astype(jnp.float32) + rms_scale(moe.astype(jnp.float32), post_ffn_gain)).astype(
        jnp.bfloat16
    )
    return (result, new_latent, new_rope)


def solution(mesh):
    return jax.shard_map(
        body,
        mesh=mesh,
        in_specs=(
            P(("ep", "tp"), None),
            P(("ep", "tp"), None, None),
            P(("ep", "tp"), None, None),
            P(("ep", "tp")),
            P(),
            P(),
            P(),
            P(),
            P(),
            P(None, "tp"),
            P(None, "tp"),
            P(None, "tp"),
            P(),
            P(None, "tp", None),
            P(None, "tp", None),
            P("tp", None),
            P("ep", None),
            P("ep", None),
            P("ep", None, "tp"),
            P("ep", None, "tp"),
            P("ep", "tp", None),
        ),
        out_specs=(P(("ep", "tp"), None), P(("ep", "tp"), None), P(("ep", "tp"), None)),
        check_vma=False,
    )
```

profile of v0, /device:TPU:0, one launch (start us, length us, event | category | flops | bytes accessed | tf_op | source)
XLA Modules:
  0.0 185.8 jit_solution(10452083939786352864)
XLA Ops:
  9.9 7.2 %all-gather = bf16[4,12,2048]{2,1,0:T(8,128)(2,1)S(1)} all-gather(bf16[1,12,2048]{2,1,0:T(8,128)(2,1)S(1)} %fusion.77), channel_id=1, replica_groups=mesh['ep'=8,'tp'=4] {'tp'}, dimensions={0}, use_global_device_ids=true | all-gather | bytes 245760 | tf_op jit(solution)/shard_map/all_gather | solution.py:118
  17.3 2.8 %fusion.46 = bf16[48,896]{1,0:T(8,128)(2,1)S(1)} fusion(bf16[48,2048]{1,0:T(8,128)(2,1)S(1)} %reshape.241, bf16[2048,128]{1,0:T(8,128)(2,1)} %param.36, bf16[2048,256]{1,0:T(8,128)(2,1)} %param.35, bf16[2048,512]{1,0:T(8,128)(2,1)} %param.34), kind=kOutput, calls=%fused_computation.36 | convolution fusion | flops 187213824 | bytes 3952640 | tf_op jit(solution)/shard_map/dot_general | solution.py:120
  20.7 3.3 %all-to-all-start.2 = ((bf16[4,12,128]{2,1,0:T(8,128)(2,1)}), bf16[4,12,128]{2,1,0:T(8,128)(2,1)S(1)}, u32[]{:S(2)}, u32[]{:S(2)}) async-start(bf16[4,12,128]{2,1,0:T(8,128)(2,1)} %all_to_all.64), calls=%async_computation.2 | async-start | bytes 32768 | tf_op jit(solution)/shard_map/all_to_all | solution.py:136
  30.1 3.3 %all-to-all-start.1 = ((bf16[4,2,1536]{2,1,0:T(2,128)(2,1)}), bf16[4,2,1536]{2,1,0:T(2,128)(2,1)S(1)}, u32[]{:S(2)}, u32[]{:S(2)}) async-start(bf16[4,2,1536]{2,1,0:T(2,128)(2,1)} %reshape.251), calls=%async_computation.1 | async-start | bytes 49152 | tf_op jit(solution)/shard_map/all_to_all | solution.py:135
  33.7 3.6 %all-to-all-done.1 = bf16[4,2,1536]{2,1,0:T(2,128)(2,1)S(1)} async-done(((bf16[4,2,1536]{2,1,0:T(2,128)(2,1)}), bf16[4,2,1536]{2,1,0:T(2,128)(2,1)S(1)}, u32[]{:S(2)}, u32[]{:S(2)}) %all-to-all-start.1) | async-done | bytes 24608 | tf_op jit(solution)/shard_map/all_to_all | solution.py:135
  37.3 3.4 %all-to-all-start = ((bf16[48,4,512]{2,1,0:T(4,128)(2,1)}), bf16[48,4,512]{2,1,0:T(4,128)(2,1)S(1)}, u32[]{:S(2)}, u32[]{:S(2)}) async-start(bf16[48,4,512]{2,1,0:T(4,128)(2,1)} %copy.133), calls=%async_computation | async-start | bytes 393216 | tf_op jit(solution)/shard_map/all_to_all | solution.py:134
  41.1 4.8 %all-to-all-done = bf16[48,4,512]{2,1,0:T(4,128)(2,1)S(1)} async-done(((bf16[48,4,512]{2,1,0:T(4,128)(2,1)}), bf16[48,4,512]{2,1,0:T(4,128)(2,1)S(1)}, u32[]{:S(2)}, u32[]{:S(2)}) %all-to-all-start) | async-done | bytes 196640 | tf_op jit(solution)/shard_map/all_to_all | solution.py:134
  46.2 9.9 %while.20 = (s32[]{:T(128)}, f32[12,16,1024]{2,1,0:T(8,128)S(1)}, s32[]{:T(128)}, bf16[12,1024,512]{2,1,0:T(8,128)(2,1)}, bf16[12,16,512]{2,1,0:T(8,128)(2,1)S(1...) while((s32[]{:T(128)}, f32[12,16,1024]{2,1,0:T(8,128)S(1)}, ...), condition=%wide.region_3.4_spmd, body=%wide.region_2.0_spmd.sunk | while | flops 113442824 | bytes 14795963 | solution.py:50
  46.2 4.6 %fusion.120 = f32[12,512,16]{1,2,0:T(8,128)S(1)} fusion(bf16[12,16,512]{2,1,0:T(8,128)(2,1)S(1)} %get-tuple-element.211, bf16[12,1024,512]{2,1,0:T(8,128)(2,1)} %get-tuple-element.210, s32[]{:T(128)S(6)} %select_n.38), kind=kOutput, calls=%fused_computation.clone.1 | convolution fusion | flops 100663296 | bytes 6881284 | tf_op jit(solution)/shard_map/while/body/shc,spc->shp/dot_general | solution.py:42
  51.1 4.6 %fusion.120 = f32[12,512,16]{1,2,0:T(8,128)S(1)} fusion(bf16[12,16,512]{2,1,0:T(8,128)(2,1)S(1)} %get-tuple-element.211, bf16[12,1024,512]{2,1,0:T(8,128)(2,1)} %get-tuple-element.210, s32[]{:T(128)S(6)} %select_n.38), kind=kOutput, calls=%fused_computation.clone.1 | convolution fusion | flops 100663296 | bytes 6881284 | tf_op jit(solution)/shard_map/while/body/shc,spc->shp/dot_general | solution.py:42
  57.0 7.5 %while.21 = (s32[]{:T(128)}, f32[12,16,512]{2,1,0:T(8,128)S(1)}, s32[]{:T(128)}, bf16[12,16,1024]{2,1,0:T(8,128)(2,1)S(1)}, bf16[12,1024,512]{2,1,0:T(8,128)(2,1...) while((s32[]{:T(128)}, f32[12,16,512]{2,1,0:T(8,128)S(1)}, s32[]{:T(128)}, ...), condition=%wide.region_8.9_spmd, body=%wide.region_7.8_spmd.sunk | while | flops 100761608 | bytes 7275659 | solution.py:74
  57.0 3.7 %fusion.124 = f32[12,16,512]{2,1,0:T(8,128)S(1)} fusion(f32[12,16,512]{2,1,0:T(8,128)S(1)} %get-tuple-element.228, bf16[12,1024,512]{2,1,0:T(8,128)(2,1)} %get-tuple-element.240, s32[]{:T(128)S(6)} %select_n.39, bf16[12,16,1024]{2,1,0:T(8,128)(2,1)S(1)} %get-tuple-element.239), kind=kOutput, calls=%fused_computation.11.clone.1 | convolution fusion | flops 100761600 | bytes 7275520 | tf_op jit(solution)/shard_map/while/body/shp,spc->shc/dot_general | solution.py:70
  60.8 3.7 %fusion.124 = f32[12,16,512]{2,1,0:T(8,128)S(1)} fusion(f32[12,16,512]{2,1,0:T(8,128)S(1)} %get-tuple-element.228, bf16[12,1024,512]{2,1,0:T(8,128)(2,1)} %get-tuple-element.240, s32[]{:T(128)S(6)} %select_n.39, bf16[12,16,1024]{2,1,0:T(8,128)(2,1)S(1)} %get-tuple-element.239), kind=kOutput, calls=%fused_computation.11.clone.1 | convolution fusion | flops 100761600 | bytes 7275520 | tf_op jit(solution)/shard_map/while/body/shp,spc->shc/dot_general | solution.py:70
  65.5 3.4 %all-to-all-start.3 = ((bf16[12,16,512]{2,0,1:T(8,128)(2,1)}), bf16[12,16,512]{2,0,1:T(8,128)(2,1)S(1)}, u32[]{:S(2)}, u32[]{:S(2)}) async-start(bf16[12,16,512]{2,0,1:T(8,128)(2,1)} %fusion.53), calls=%async_computation.3 | async-start | bytes 524288 | tf_op jit(solution)/shard_map/all_to_all | solution.py:145
  69.0 5.9 %all-to-all-done.3 = bf16[12,16,512]{2,0,1:T(8,128)(2,1)S(1)} async-done(((bf16[12,16,512]{2,0,1:T(8,128)(2,1)}), bf16[12,16,512]{2,0,1:T(8,128)(2,1)S(1)}, u32[]{:S(2)}, u32[]{:S(2)}) %all-to-all-start.3) | async-done | bytes 196640 | tf_op jit(solution)/shard_map/all_to_all | solution.py:145
  78.4 8.6 %fusion = bf16[16,2048]{1,0:T(8,128)(2,1)S(1)} fusion(bf16[48,2048]{1,0:T(8,128)(2,1)S(1)} %convolution_convert_fusion.2), kind=kCustom, calls=%all-reduce-scatter | all-reduce-scatter fusion | flops 131073 | bytes 262656
  90.5 8.0 %all-gather.1 = bf16[4,12,2048]{2,1,0:T(8,128)(2,1)S(1)} all-gather(bf16[1,12,2048]{2,1,0:T(8,128)(2,1)S(1)} %fusion.68), channel_id=1, replica_groups=mesh['ep'=8,'tp'=4] {'tp'}, dimensions={0}, use_global_device_ids=true | all-gather | bytes 245760 | tf_op jit(solution)/shard_map/all_gather | solution.py:158
  101.2 14.1 %all_to_all.81 = bf16[8,25,512]{2,1,0:T(8,128)(2,1)S(1)} all-to-all(bf16[8,25,512]{2,1,0:T(8,128)(2,1)S(1)} %constant_dynamic-slice_fusion), channel_id=1, replica_groups=mesh['ep'=8,'tp'=4] {'ep'}, dimensions={0} | all-to-all | bytes 409600 | tf_op jit(solution)/shard_map/all_to_all | solution.py:178
  115.2 10.0 %all_gather.11 = bf16[8,25,2048]{2,1,0:T(8,128)(2,1)S(1)} all-gather(bf16[8,25,512]{2,1,0:T(8,128)(2,1)S(1)} %all_to_all.81), channel_id=1, replica_groups=mesh['ep'=8,'tp'=4] {'tp'}, dimensions={2}, use_global_device_ids=true | all-gather | bytes 1024000 | tf_op jit(solution)/shard_map/all_gather | solution.py:177
  131.7 23.6 %reduce-scatter.4.cloned.1.call-done = bf16[8,25,512]{2,1,0:T(8,128)(2,1)} async-done(((bf16[8,25,2048]{2,1,0:T(8,128)(2,1)}), bf16[8,25,512]{2,1,0:T(8,128)(2,1)}) %reduce-scatter.4.cloned.1.call-update) | async-done | bytes 204816 | tf_op jit(solution)/shard_map/reduce_scatter | solution.py:192
  155.3 5.5 %all-to-all-start.5 = ((bf16[8,25,512]{2,1,0:T(8,128)(2,1)}), bf16[8,25,512]{2,1,0:T(8,128)(2,1)S(1)}, u32[]{:S(2)}, u32[]{:S(2)}) async-start(bf16[8,25,512]{2,1,0:T(8,128)(2,1)} %reduce-scatter.4.cloned.1.call-done), calls=%async_computation.6 | async-start | bytes 524288 | tf_op jit(solution)/shard_map/all_to_all | solution.py:195
  161.0 8.6 %all-to-all-done.5 = bf16[8,25,512]{2,1,0:T(8,128)(2,1)S(1)} async-done(((bf16[8,25,512]{2,1,0:T(8,128)(2,1)}), bf16[8,25,512]{2,1,0:T(8,128)(2,1)S(1)}, u32[]{:S(2)}, u32[]{:S(2)}) %all-to-all-start.5) | async-done | bytes 204832 | tf_op jit(solution)/shard_map/all_to_all | solution.py:195
  170.5 3.3 %all-to-all-start.6 = ((bf16[4,12,512]{2,1,0:T(8,128)(2,1)}), bf16[4,12,512]{2,1,0:T(8,128)(2,1)S(1)}, u32[]{:S(2)}, u32[]{:S(2)}) async-start(bf16[4,12,512]{2,1,0:T(8,128)(2,1)} %all_to_all.72), calls=%async_computation.7 | async-start | bytes 131072 | tf_op jit(solution)/shard_map/all_to_all | solution.py:203
  174.5 3.4 %all-to-all-done.6 = bf16[4,12,512]{2,1,0:T(8,128)(2,1)S(1)} async-done(((bf16[4,12,512]{2,1,0:T(8,128)(2,1)}), bf16[4,12,512]{2,1,0:T(8,128)(2,1)S(1)}, u32[]{:S(2)}, u32[]{:S(2)}) %all-to-all-start.6) | async-done | bytes 49184 | tf_op jit(solution)/shard_map/all_to_all | solution.py:203
  (134 shorter events, 30.2 us)
Async XLA Ops:
  7.2 122.7 %copy-start = (bf16[1,512,2048]{2,1,0:T(8,128)(2,1)S(1)}, bf16[1,512,2048]{2,1,0:T(8,128)(2,1)}, u32[]{:S(2)}) copy-start(bf16[1,512,2048]{2,1,0:T(8,128)(2,1)} %param.45) | copy-start | bytes 6291460
  17.2 6.8 %copy-start.12 = (s32[12]{0:T(128)S(1)}, s32[12]{0:T(128)}, u32[]{:S(2)}) copy-start(s32[12]{0:T(128)} %param.28) | copy-start | bytes 148
  17.2 7.5 %copy-start.3 = (bf16[12,2048]{1,0:T(8,128)(2,1)S(1)}, bf16[12,2048]{1,0:T(8,128)(2,1)}, u32[]{:S(2)}) copy-start(bf16[12,2048]{1,0:T(8,128)(2,1)} %param.25) | copy-start | bytes 147460
  17.2 8.7 %copy-start.4 = (bf16[512,4,128]{2,1,0:T(4,128)(2,1)S(1)}, bf16[512,4,128]{2,1,0:T(4,128)(2,1)}, u32[]{:S(2)}) copy-start(bf16[512,4,128]{2,1,0:T(4,128)(2,1)} %param.38) | copy-start | bytes 1572868
  17.2 9.0 %copy-start.7 = (s32[48,4]{0,1:T(4,128)S(1)}, s32[48,4]{0,1:T(4,128)}, u32[]{:S(2)}) copy-start(s32[48,4]{0,1:T(4,128)} %param.42) | copy-start | bytes 2308
  17.2 12.7 %copy-start.11 = (bf16[512]{0:T(512)(128)(2,1)S(1)}, bf16[512]{0:T(512)(128)(2,1)}, u32[]{:S(2)}) copy-start(bf16[512]{0:T(512)(128)(2,1)} %param.30) | copy-start | bytes 3076
  20.7 9.4 %all-to-all-start.2 = ((bf16[4,12,128]{2,1,0:T(8,128)(2,1)}), bf16[4,12,128]{2,1,0:T(8,128)(2,1)S(1)}, u32[]{:S(2)}, u32[]{:S(2)}) async-start(bf16[4,12,128]{2,1,0:T(8,128)(2,1)} %all_to_all.64), calls=%async_computation.2 | async-start | bytes 32768 | tf_op jit(solution)/shard_map/all_to_all | solution.py:136
  30.1 7.2 %all-to-all-start.1 = ((bf16[4,2,1536]{2,1,0:T(2,128)(2,1)}), bf16[4,2,1536]{2,1,0:T(2,128)(2,1)S(1)}, u32[]{:S(2)}, u32[]{:S(2)}) async-start(bf16[4,2,1536]{2,1,0:T(2,128)(2,1)} %reshape.251), calls=%async_computation.1 | async-start | bytes 49152 | tf_op jit(solution)/shard_map/all_to_all | solution.py:135
  33.7 22.4 %copy-start.6 = (bf16[12,512]{1,0:T(8,128)(2,1)}, bf16[12,512]{1,0:T(8,128)(2,1)S(1)}, u32[]{:S(2)}) copy-start(bf16[12,512]{1,0:T(8,128)(2,1)S(1)} %get-tuple-element.98) | copy-start | bytes 36868
  37.3 8.6 %all-to-all-start = ((bf16[48,4,512]{2,1,0:T(4,128)(2,1)}), bf16[48,4,512]{2,1,0:T(4,128)(2,1)S(1)}, u32[]{:S(2)}, u32[]{:S(2)}) async-start(bf16[48,4,512]{2,1,0:T(4,128)(2,1)} %copy.133), calls=%async_computation | async-start | bytes 393216 | tf_op jit(solution)/shard_map/all_to_all | solution.py:134
  46.2 4.7 %copy-start.1 = (bf16[12,64,1024]{2,1,0:T(8,128)(2,1)S(1)}, bf16[12,64,1024]{2,1,0:T(8,128)(2,1)}, u32[]{:S(2)}) copy-start(bf16[12,64,1024]{2,1,0:T(8,128)(2,1)} %get-tuple-element.212) | copy-start | bytes 4718596 | tf_op jit(solution)/shard_map/while
  51.1 4.7 %copy-start.1 = (bf16[12,64,1024]{2,1,0:T(8,128)(2,1)S(1)}, bf16[12,64,1024]{2,1,0:T(8,128)(2,1)}, u32[]{:S(2)}) copy-start(bf16[12,64,1024]{2,1,0:T(8,128)(2,1)} %get-tuple-element.212) | copy-start | bytes 4718596 | tf_op jit(solution)/shard_map/while
  65.5 9.4 %all-to-all-start.3 = ((bf16[12,16,512]{2,0,1:T(8,128)(2,1)}), bf16[12,16,512]{2,0,1:T(8,128)(2,1)S(1)}, u32[]{:S(2)}, u32[]{:S(2)}) async-start(bf16[12,16,512]{2,0,1:T(8,128)(2,1)} %fusion.53), calls=%async_computation.3 | async-start | bytes 524288 | tf_op jit(solution)/shard_map/all_to_all | solution.py:145
  68.9 19.6 %copy-start.8 = (bf16[2048]{0:T(1024)(128)(2,1)S(1)}, bf16[2048]{0:T(1024)(128)(2,1)}, u32[]{:S(2)}) copy-start(bf16[2048]{0:T(1024)(128)(2,1)} %param.31) | copy-start | bytes 12292
  68.9 19.6 %copy-start.9 = (bf16[2048]{0:T(1024)(128)(2,1)S(1)}, bf16[2048]{0:T(1024)(128)(2,1)}, u32[]{:S(2)}) copy-start(bf16[2048]{0:T(1024)(128)(2,1)} %param.32) | copy-start | bytes 12292
  68.9 19.6 %copy-start.13 = (u32[32]{0:T(128)S(1)}, u32[32]{0:T(128)}, u32[]{:S(2)}) copy-start(u32[32]{0:T(128)} %constant.101) | copy-start | bytes 388
  68.9 86.3 %reduce-scatter.4.cloned.1.call-start = ((), (), s32[]{:S(2)}) async-start(), calls=%async_computation.8 | async-start | bytes 1310720 | tf_op jit(solution)/shard_map/reduce_scatter | solution.py:192
  87.0 2.7 %collective-permute-start = (bf16[12,2048]{1,0:T(8,128)(2,1)S(1)}, bf16[12,2048]{1,0:T(8,128)(2,1)S(1)}, u32[]{:S(2)}, u32[]{:S(2)}) collective-permute-start(bf16[12,2048]{1,0:T(8,128)(2,1)S(1)} %slice.49), channel_id=1, source_target_pairs={{0,1},{1,2},{2,3},{4,5},{5,6},{6,7},{8,9},{9,10},{10,11},{12,13},{... | collective-permute-start | bytes 147464
  126.5 2.6 %copy-start.2 = (bf16[200,2048]{1,0:T(8,128)(2,1)S(1)}, bf16[200,2048]{1,0:T(8,128)(2,1)}, u32[]{:S(2)}) copy-start(bf16[200,2048]{1,0:T(8,128)(2,1)} %reshape.233) | copy-start | bytes 2457604
  126.5 2.7 %copy-start.14 = (bf16[1,2048,512]{2,1,0:T(8,128)(2,1)S(1)}, bf16[1,2048,512]{2,1,0:T(8,128)(2,1)}, u32[]{:S(2)}) copy-start(bf16[1,2048,512]{2,1,0:T(8,128)(2,1)} %param.44) | copy-start | bytes 6291460
  129.9 1.7 copy-start.5
  131.6 42.8 %copy-start.10 = (bf16[2048]{0:T(1024)(128)(2,1)S(1)}, bf16[2048]{0:T(1024)(128)(2,1)}, u32[]{:S(2)}) copy-start(bf16[2048]{0:T(1024)(128)(2,1)} %param.33) | copy-start | bytes 12292
  155.3 14.3 %all-to-all-start.5 = ((bf16[8,25,512]{2,1,0:T(8,128)(2,1)}), bf16[8,25,512]{2,1,0:T(8,128)(2,1)S(1)}, u32[]{:S(2)}, u32[]{:S(2)}) async-start(bf16[8,25,512]{2,1,0:T(8,128)(2,1)} %reduce-scatter.4.cloned.1.call-done), calls=%async_computation.6 | async-start | bytes 524288 | tf_op jit(solution)/shard_map/all_to_all | solution.py:195
  170.5 7.4 %all-to-all-start.6 = ((bf16[4,12,512]{2,1,0:T(8,128)(2,1)}), bf16[4,12,512]{2,1,0:T(8,128)(2,1)S(1)}, u32[]{:S(2)}, u32[]{:S(2)}) async-start(bf16[4,12,512]{2,1,0:T(8,128)(2,1)} %all_to_all.72), calls=%async_computation.7 | async-start | bytes 131072 | tf_op jit(solution)/shard_map/all_to_all | solution.py:203
Sparse Core Ops, SparseCore 0:
  131.8 23.4 reduce-scatter.3
where the time goes:
time: 187 us; the launch traced here: 186 us
  waiting for transfers between devices  49.9 us (27%)
  blocking collectives  47.9 us (26%)
  matrix products  30.7 us (16%)
  starting transfers between devices  23.4 us (13%)
  between operations  16 us (9%)
  local copies, waits for them, and re-layouts  8.94 us (5%)
  other arithmetic  8.78 us (5%)
    reduce_scatter x1, waiting for transfers between devices, body(): lax.psum_scatter(partial_out.astype(jnp.bfloat16), 'tp', scatter_dimensio...  23.6 us
    all_to_all x1, blocking collectives, body(): lax.all_to_all(sent, 'ep', split_axis=0, concat_axis=0, tiled=True)  14.1 us
    all_gather x1, blocking collectives, body(): lax.all_gather(lax.all_to_all(sent, 'ep', split_axis=0, concat_axis=0, ti...  10 us
    dot_general x2, matrix products, score_block(): jnp.einsum('shc,spc->shp', query_latent, latents, preferred_element_type=...  9.29 us
    unnamed x1, blocking collectives  8.63 us
    all_to_all x1, waiting for transfers between devices, body(): lax.all_to_all(summed, 'ep', split_axis=0, concat_axis=0, tiled=True)  8.57 us
    all_gather x1, blocking collectives, body(): group_inputs = lax.all_gather(ffn_input, 'tp', axis=0, tiled=True)  7.98 us
    dot_general x2, matrix products, read_block(): jnp.einsum('shp,spc->shc', weights, latents, preferred_element_type=jnp.f...  7.44 us
  transfers between devices with their start and end apart: 8, of which 6 were waited for; matrix products, arithmetic and copies ran while one was open for 4% of the time, Pallas kernels for 0%

commit v1 on v0

v1 whole, which is shorter than its diff:
```python
import functools

import jax
import jax.numpy as jnp
from jax import lax
from jax.experimental import pallas as pl
from jax.experimental.pallas import tpu as pltpu
from jax.sharding import PartitionSpec as P

eps_norm = 1e-06
clamp_limit = 7.0
sigmoid_alpha = 1.702
theta_base = 10000.0
MESH = pl.DeviceIdType.MESH
F32 = jnp.float32
BF16 = jnp.bfloat16


def rms_scale(values, gain):
    mean_square = jnp.mean(values * values, axis=-1, keepdims=True)
    return values * lax.rsqrt(mean_square + eps_norm) * gain


def turn(values, cosine, sine):
    half = values.shape[-1] // 2
    swapped = jnp.concatenate([values[:, half:], values[:, :half]], axis=1)
    return values * cosine + swapped * sine


def dot(a, b):
    return jnp.dot(a, b, preferred_element_type=F32)


def dot_nt(a, b):
    return lax.dot_general(a, b, (((1,), (1,)), ((), ())), preferred_element_type=F32)


def remote(src, dst, send_sem, recv_sem, where):
    return pltpu.make_async_remote_copy(
        src_ref=src,
        dst_ref=dst,
        send_sem=send_sem,
        recv_sem=recv_sem,
        device_id=where,
        device_id_type=MESH,
    )


def kernel(
    cfg,
    lengths,
    tokens,
    gains,
    latent_gain,
    cosine,
    sine,
    routes,
    routes_t,
    logits,
    cache_h,
    rope_h,
    wq_h,
    wqr_h,
    wl_h,
    wkr_h,
    wku_h,
    wvu_h,
    wo_h,
    wg_h,
    wu_h,
    wd_h,
    out_result,
    out_latent,
    out_rope,
    cache,
    rope,
    wq,
    wqr,
    wl,
    wkr,
    wku,
    wvu,
    wo,
    wg,
    wu,
    wd,
    xg,
    qsend,
    qrecv,
    qs,
    qt,
    nlat,
    nrope,
    hl,
    hsend,
    hrecv,
    asend,
    arecv,
    fg,
    sl,
    xr,
    act,
    part,
    s1,
    xsend,
    xrecv,
    rsend,
    ret,
    msend,
    mrecv,
    w_sem,
    c_sem,
    r_sem,
    tp_send,
    tp_recv,
    own_sem,
    d_send,
    d_recv,
    x_send,
    x_recv,
    sib_send,
    sib_recv,
    s1_send,
    s1_recv,
    rx_send,
    rx_recv,
    ret_send,
    ret_recv,
):
    T, EP, R, RP, LH, CP, scale = cfg
    H = T * LH
    t = lax.axis_index("tp")
    e = lax.axis_index("ep")
    C = wku.shape[0]
    KD = wq.shape[1] // LH
    RD = wkr.shape[1]
    VD = wvu.shape[1] // LH
    LC = wl.shape[1]
    D = wq.shape[0]
    Q = D // T
    G = T * RP
    S = EP * CP
    SPAN = cache.shape[1]
    sib = t + 1 - 2 * lax.rem(t, 2)

    loads = {}
    for i, (name, src, dst) in enumerate(
        [
            ("wq", wq_h, wq),
            ("wqr", wqr_h, wqr),
            ("wl", wl_h, wl),
            ("wkr", wkr_h, wkr),
            ("wku", wku_h, wku),
            ("wvu", wvu_h, wvu),
            ("wo", wo_h, wo),
            ("wg", wg_h.at[0], wg),
            ("wu", wu_h.at[0], wu),
            ("wd", wd_h.at[0], wd),
        ]
    ):
        loads[name] = pltpu.make_async_copy(src, dst, w_sem.at[i])
    for name in ("wq", "wqr", "wl", "wkr", "wku"):
        loads[name].start()

    barrier = pltpu.get_barrier_semaphore()
    for k in range(1, T):
        pl.semaphore_signal(
            barrier, inc=1, device_id={"tp": lax.rem(t + k, T)}, device_id_type=MESH
        )
    for k in range(1, EP):
        pl.semaphore_signal(
            barrier, inc=1, device_id={"ep": lax.rem(e + k, EP)}, device_id_type=MESH
        )

    def cache_copy(b):
        return pltpu.make_async_copy(cache_h.at[b], cache.at[b], c_sem.at[b])

    def rope_copy(b):
        return pltpu.make_async_copy(rope_h.at[b], rope.at[b], r_sem.at[b])

    token_values = tokens[...].astype(F32)
    xg[t] = rms_scale(token_values, gains[0:1, :]).astype(BF16)
    pl.semaphore_wait(barrier, T - 1 + EP - 1)

    def gather_tp(phase, buf):
        copies = []
        for k in range(1, T):
            c = remote(
                buf.at[t],
                buf.at[t],
                tp_send.at[phase, k],
                tp_recv.at[phase, k],
                {"tp": lax.rem(t + k, T)},
            )
            c.start()
            copies.append(c)
        return copies

    def scatter_tp(phase, src, dst):
        copies = []
        for k in range(1, T):
            peer = lax.rem(t + k, T)
            c = remote(
                src.at[peer],
                dst.at[t],
                tp_send.at[phase, k],
                tp_recv.at[phase, k],
                {"tp": peer},
            )
            c.start()
            copies.append(c)
        dst[t] = src[t]
        return copies

    def finish(copies):
        for c in copies:
            c.wait()

    copies = gather_tp(0, xg)
    for b in range(R):
        cache_copy(b).start()
        rope_copy(b).start()
    loads["wkr"].wait()
    key_raw = dot(xg[t], wkr[...]).astype(BF16).astype(F32)
    new_rope = turn(key_raw, cosine[...], sine[...]).astype(BF16)
    nrope[...] = new_rope.astype(F32)
    out_rope[...] = new_rope[:R]
    for name in ("wq", "wqr", "wl", "wku"):
        loads[name].wait()
    finish(copies)

    rows = xg[...].reshape(G, D)
    plain = dot(rows, wq[...]).astype(BF16)
    rotary = dot(rows, wqr[...]).astype(BF16)
    latent_part = dot(rows, wl[...]).astype(BF16)
    for h in range(LH):
        lat = dot_nt(plain[:, h * KD : (h + 1) * KD], wku[:, h * KD : (h + 1) * KD])
        qsend[:, :, h * C : (h + 1) * C] = lat.astype(BF16).reshape(T, RP, C)
    base = LH * C
    qsend[:, :, base : base + LH * RD] = rotary.reshape(T, RP, LH * RD)
    qsend[:, :, base + LH * RD :] = latent_part.reshape(T, RP, LC)
    copies = scatter_tp(1, qsend, qrecv)
    for name in ("wvu", "wo", "wg", "wu", "wd"):
        loads[name].start()
    ri = lax.broadcasted_iota(jnp.int32, (RP * H, RP * H), 0)
    ci = lax.broadcasted_iota(jnp.int32, (RP * H, RP * H), 1)
    head_shift = H.bit_length() - 1
    row_shift = RP.bit_length() - 1
    to_seq = (
        ci == ((ri & (H - 1)) << row_shift) + (ri >> head_shift)
    ).astype(F32).astype(BF16)
    to_head = (
        ci == ((ri & (RP - 1)) << head_shift) + (ri >> row_shift)
    ).astype(F32).astype(BF16)
    finish(copies)

    latent_raw = jnp.concatenate(
        [qrecv[s, :, base + LH * RD :] for s in range(T)], axis=1
    ).astype(F32)
    new_latent = rms_scale(latent_raw, latent_gain[...]).astype(BF16)
    out_latent[...] = new_latent[:R]
    nlat[...] = new_latent.astype(F32)
    stacked = jnp.concatenate(
        [qrecv[s, :, h * C : (h + 1) * C] for s in range(T) for h in range(LH)], axis=0
    )
    qs[...] = dot(to_seq, stacked).astype(BF16).reshape(RP, H, C)
    turned = jnp.concatenate(
        [
            turn(
                qrecv[s, :, base + h * RD : base + (h + 1) * RD].astype(F32),
                cosine[...],
                sine[...],
            ).astype(BF16)
            for s in range(T)
            for h in range(LH)
        ],
        axis=0,
    )
    qt[...] = dot(to_seq, turned).astype(BF16).reshape(RP, H, RD)
    if RP > R:
        hl[R:] = jnp.zeros((RP - R, H, C), BF16)

    def attend(b, carry):
        cache_copy(b).wait()
        rope_copy(b).wait()
        q = qs[b]
        qr = qt[b]
        latents = cache[b]
        fresh = nlat[pl.ds(b, 1), :]
        fresh_rope = nrope[pl.ds(b, 1), :]
        scores = (dot_nt(q, latents) + dot(qr, rope[b])) * scale
        own = (
            jnp.sum(q.astype(F32) * fresh, axis=1, keepdims=True)
            + jnp.sum(qr.astype(F32) * fresh_rope, axis=1, keepdims=True)
        ) * scale
        valid = lax.broadcasted_iota(jnp.int32, (H, SPAN), 1) < lengths[b]
        masked = jnp.where(valid, scores, -1e30)
        highest = jnp.maximum(jnp.max(masked, axis=1, keepdims=True), own)
        raised = jnp.where(valid, jnp.exp(masked - highest), 0.0)
        raised_own = jnp.exp(own - highest)
        total = jnp.sum(raised, axis=1, keepdims=True) + raised_own
        inverse = 1.0 / total
        probs = (raised * inverse).astype(BF16)
        prob_own = (raised_own * inverse).astype(BF16).astype(F32)
        hl[b] = (dot(probs, latents) + prob_own * fresh).astype(BF16)
        return carry

    lax.fori_loop(0, R, attend, 0)

    by_head = dot(to_head, hl[...].reshape(RP * H, C)).astype(BF16)
    hsend[...] = by_head.reshape(T, LH * RP, C)
    copies = scatter_tp(2, hsend, hrecv)
    loads["wvu"].wait()
    loads["wo"].wait()

    slot_shift = CP.bit_length() - 1
    s_lane = lax.broadcasted_iota(jnp.int32, (G, S), 1)
    e_lane = s_lane >> slot_shift
    c_lane = (s_lane & (CP - 1)).astype(F32)
    s_sub = lax.broadcasted_iota(jnp.int32, (S, G), 0)
    e_sub = s_sub >> slot_shift
    c_sub = (s_sub & (CP - 1)).astype(F32)
    gi = lax.broadcasted_iota(jnp.int32, (G, G), 0)
    gj = lax.broadcasted_iota(jnp.int32, (G, G), 1)
    lower = (gj < gi).astype(F32).astype(BF16)
    upper = (gi < gj).astype(F32).astype(BF16)
    K = routes.shape[1]
    lg = logits[...]
    lg = jnp.exp(lg - jnp.max(lg, axis=1, keepdims=True))
    weights = lg / jnp.sum(lg, axis=1, keepdims=True)
    count = jnp.zeros((G, S), F32)
    weighted = jnp.zeros((G, S), F32)
    count_t = jnp.zeros((S, G), F32)
    for k in range(K):
        hit = routes[:, k : k + 1] == e_lane
        count = jnp.where(hit, 1.0, count)
        weighted = jnp.where(hit, weights[:, k : k + 1], weighted)
        count_t = jnp.where(routes_t[k : k + 1, :] == e_sub, 1.0, count_t)
    rank = dot(lower, count.astype(BF16))
    rank_t = dot(count_t.astype(BF16), upper)
    combine = jnp.where(rank == c_lane, weighted, 0.0)
    combine_hi = combine.astype(BF16)
    combine_lo = (combine - combine_hi.astype(F32)).astype(BF16)
    dispatch = jnp.where(rank_t == c_sub, count_t, 0.0).astype(BF16)

    finish(copies)
    values = []
    for h in range(LH):
        mine = jnp.concatenate(
            [hrecv[s, h * RP : (h + 1) * RP, :] for s in range(T)], axis=0
        )
        values.append(dot(mine, wvu[:, h * VD : (h + 1) * VD]).astype(BF16))
    values = jnp.concatenate(values, axis=1)
    asend[...] = dot(values, wo[...]).astype(BF16).reshape(T, RP, D)
    finish(scatter_tp(3, asend, arecv))
    attn = arecv[0].astype(F32)
    for s in range(1, T):
        attn = attn + arecv[s].astype(F32)
    attn = attn.astype(BF16).astype(F32)
    mixed = (token_values + rms_scale(attn, gains[1:2, :])).astype(BF16).astype(F32)
    fg[t] = rms_scale(mixed, gains[2:3, :]).astype(BF16)
    finish(gather_tp(4, fg))

    mine = fg[:, :, pl.ds(pl.multiple_of(t * Q, Q), Q)].reshape(G, Q)
    sl[...] = dot(dispatch, mine).astype(BF16).reshape(EP, CP, Q)
    sent = [None]
    for k in range(1, EP):
        peer = lax.rem(e + k, EP)
        c = remote(sl.at[peer], xr.at[t, e], d_send.at[k], d_recv.at[k], {"ep": peer})
        c.start()
        sent.append(c)
    xr[t, e] = sl[e]
    pairs = T // 2
    across = []
    to_sib = []
    for k in range(EP):
        src = lax.rem(e + EP - k, EP)
        if k:
            sent[k].wait_recv()
        row = []
        for j in range(1, pairs):
            c = remote(
                xr.at[t, src],
                xr.at[t, src],
                x_send.at[k, j],
                x_recv.at[k, j],
                {"tp": lax.rem(t + 2 * j, T)},
            )
            c.start()
            row.append(c)
        across.append(row)
        c = remote(
            xr.at[t, src], xr.at[t, src], sib_send.at[k, 0], sib_recv.at[k, 0], {"tp": sib}
        )
        c.start()
        to_sib.append(c)
    for k in range(EP):
        src = lax.rem(e + EP - k, EP)
        for j in range(1, pairs):
            across[k][j - 1].wait_recv()
            quarter = lax.rem(t + T - 2 * j, T)
            c = remote(
                xr.at[quarter, src],
                xr.at[quarter, src],
                sib_send.at[k, j],
                sib_recv.at[k, j],
                {"tp": sib},
            )
            c.start()
            to_sib.append(c)
    for name in ("wg", "wu", "wd"):
        loads[name].wait()
    for c in to_sib:
        c.wait_recv()

    gate = jnp.zeros((S, wg.shape[1]), F32)
    upward = jnp.zeros((S, wg.shape[1]), F32)
    for q in range(T):
        block = xr[q].reshape(S, Q)
        gate = gate + dot(block, wg[q * Q : (q + 1) * Q, :])
        upward = upward + dot(block, wu[q * Q : (q + 1) * Q, :])
    gate = jnp.minimum(gate, clamp_limit)
    upward = jnp.clip(upward, -clamp_limit, clamp_limit)
    active = (upward + 1.0) * gate * (1.0 / (1.0 + jnp.exp(-sigmoid_alpha * gate)))
    act[...] = active.astype(BF16)

    halves = []
    for j in range(pairs - 1, -1, -1):
        quarter = lax.rem(sib + 2 * j, T)
        cols = pl.ds(pl.multiple_of(quarter * Q, Q), Q)
        part[quarter] = dot(act[...], wd[:, cols]).astype(BF16).reshape(EP, CP, Q)
        c = remote(
            part.at[quarter], s1.at[quarter], s1_send.at[j], s1_recv.at[j], {"tp": sib}
        )
        c.start()
        halves.append((j, c))
    for j in range(pairs - 1, -1, -1):
        quarter = lax.rem(t + 2 * j, T)
        cols = pl.ds(pl.multiple_of(quarter * Q, Q), Q)
        part[quarter] = dot(act[...], wd[:, cols]).astype(BF16).reshape(EP, CP, Q)
    reduced = [[None] * pairs for _ in range(EP)]
    order = list(range(1, EP)) + [0]
    for j, c in halves:
        c.wait_recv()
        if j == 0:
            continue
        quarter = lax.rem(t + 2 * j, T)
        for k in order:
            src = lax.rem(e + EP - k, EP)
            both = part[quarter, src].astype(F32) + s1[quarter, src].astype(F32)
            xsend[j, src] = both.astype(BF16)
            cc = remote(
                xsend.at[j, src],
                xrecv.at[j, src],
                rx_send.at[k, j],
                rx_recv.at[k, j],
                {"tp": quarter},
            )
            cc.start()
            reduced[k][j] = cc
    back = []
    for k in order:
        src = lax.rem(e + EP - k, EP)
        total = part[t, src].astype(F32) + s1[t, src].astype(F32)
        for j in range(1, pairs):
            reduced[k][j].wait_recv()
            total = total + xrecv[j, src].astype(F32)
        if k:
            rsend[src] = total.astype(BF16)
            c = remote(rsend.at[src], ret.at[e], ret_send.at[k], ret_recv.at[k], {"ep": src})
            c.start()
            back.append(c)
        else:
            ret[e] = total.astype(BF16)
    for c in back:
        c.wait_recv()
    returned = ret[...].reshape(S, Q)
    moe_part = dot(combine_hi, returned) + dot(combine_lo, returned)
    msend[...] = moe_part.astype(BF16).reshape(T, RP, Q)
    finish(scatter_tp(5, msend, mrecv))
    moe = jnp.concatenate([mrecv[s] for s in range(T)], axis=1).astype(F32)
    out_result[...] = (mixed + rms_scale(moe, gains[3:4, :])).astype(BF16)[:R]

    for c in sent[1:] + to_sib + [c for row in across for c in row] + back:
        c.wait_send()
    for _, c in halves:
        c.wait_send()
    for row in reduced:
        for c in row[1:]:
            c.wait_send()


def body(
    tokens,
    cache_latent,
    cache_rope,
    lengths,
    attn_gain,
    latent_gain,
    post_attn_gain,
    ffn_gain,
    post_ffn_gain,
    w_query,
    w_query_rot,
    w_latent,
    w_key_rot,
    w_key_up,
    w_value_up,
    w_out,
    route_logits,
    routes,
    w_gate,
    w_up,
    w_down,
):
    R, D = tokens.shape
    T = lax.axis_size("tp")
    EP = lax.axis_size("ep")
    C, LH, KD = w_key_up.shape
    RD = w_key_rot.shape[1]
    VD = w_value_up.shape[2]
    H = T * LH
    K = routes.shape[1]
    scale = (KD + RD) ** (-0.5)
    RP = 16
    while RP < R:
        RP *= 2
    cap = (R * T * K + EP - 1) // EP + 1
    CP = 16
    while CP < cap:
        CP *= 2
    Q = D // T
    F = w_gate.shape[2]
    LC = w_latent.shape[1]
    SPAN = cache_latent.shape[1]

    padded = jnp.pad(tokens, ((0, RP - R), (0, 0)))
    gains = jnp.stack([attn_gain, post_attn_gain, ffn_gain, post_ffn_gain]).astype(F32)
    half = RD // 2
    freqs = theta_base ** (-jnp.arange(half, dtype=F32) / half)
    angles = jnp.pad(lengths, (0, RP - R)).astype(F32)[:, None] * freqs
    cosine = jnp.cos(angles)
    sine = jnp.sin(angles)
    cosine = jnp.concatenate([cosine, cosine], axis=1)
    sine = jnp.concatenate([-sine, sine], axis=1)
    rt = jnp.pad(routes.reshape(T, R, K), ((0, 0), (0, RP - R), (0, 0)), constant_values=-1)
    rt = rt.reshape(T * RP, K)
    lg = jnp.pad(route_logits.reshape(T, R, K), ((0, 0), (0, RP - R), (0, 0)))
    lg = lg.reshape(T * RP, K)

    vm = pl.BlockSpec(memory_space=pltpu.VMEM)
    hbm = pl.BlockSpec(memory_space=pl.ANY)
    dma = pltpu.SemaphoreType.DMA
    pairs = T // 2
    QW = LH * C + LH * RD + LC

    def v(*shape, dtype=BF16):
        return pltpu.VMEM(shape, dtype)

    cfg = (T, EP, R, RP, LH, CP, scale)
    return pl.pallas_call(
        functools.partial(kernel, cfg),
        out_shape=(
            jax.ShapeDtypeStruct((R, D), BF16),
            jax.ShapeDtypeStruct((R, C), BF16),
            jax.ShapeDtypeStruct((R, RD), BF16),
        ),
        in_specs=[pl.BlockSpec(memory_space=pltpu.SMEM)] + [vm] * 8 + [hbm] * 12,
        out_specs=(vm, vm, vm),
        scratch_shapes=[
            v(R, SPAN, C),
            v(R, RD, SPAN),
            v(D, LH * KD),
            v(D, LH * RD),
            v(D, LC),
            v(D, RD),
            v(C, LH * KD),
            v(C, LH * VD),
            v(LH * VD, D),
            v(D, F),
            v(D, F),
            v(F, D),
            v(T, RP, D),
            v(T, RP, QW),
            v(T, RP, QW),
            v(RP, H, C),
            v(RP, H, RD),
            v(RP, C, dtype=F32),
            v(RP, RD, dtype=F32),
            v(RP, H, C),
            v(T, LH * RP, C),
            v(T, LH * RP, C),
            v(T, RP, D),
            v(T, RP, D),
            v(T, RP, D),
            v(EP, CP, Q),
            v(T, EP, CP, Q),
            v(EP * CP, F),
            v(T, EP, CP, Q),
            v(T, EP, CP, Q),
            v(pairs, EP, CP, Q),
            v(pairs, EP, CP, Q),
            v(EP, CP, Q),
            v(EP, CP, Q),
            v(T, RP, Q),
            v(T, RP, Q),
            dma((10,)),
            dma((R,)),
            dma((R,)),
            dma((6, T)),
            dma((6, T)),
            dma((1,)),
            dma((EP,)),
            dma((EP,)),
            dma((EP, pairs)),
            dma((EP, pairs)),
            dma((EP, pairs)),
            dma((EP, pairs)),
            dma((pairs,)),
            dma((pairs,)),
            dma((EP, pairs)),
            dma((EP, pairs)),
            dma((EP,)),
            dma((EP,)),
        ],
        compiler_params=pltpu.CompilerParams(
            collective_id=0, has_side_effects=True, vmem_limit_bytes=60 * 1024 * 1024
        ),
    )(
        lengths,
        padded,
        gains,
        latent_gain.astype(F32)[None, :],
        cosine,
        sine,
        rt,
        rt.T,
        lg,
        cache_latent,
        cache_rope,
        w_query,
        w_query_rot,
        w_latent,
        w_key_rot,
        w_key_up.reshape(C, LH * KD),
        w_value_up.reshape(C, LH * VD),
        w_out,
        w_gate,
        w_up,
        w_down,
    )


def solution(mesh):
    return jax.shard_map(
        body,
        mesh=mesh,
        in_specs=(
            P(("ep", "tp"), None),
            P(("ep", "tp"), None, None),
            P(("ep", "tp"), None, None),
            P(("ep", "tp")),
            P(),
            P(),
            P(),
            P(),
            P(),
            P(None, "tp"),
            P(None, "tp"),
            P(None, "tp"),
            P(),
            P(None, "tp", None),
            P(None, "tp", None),
            P("tp", None),
            P("ep", None),
            P("ep", None),
            P("ep", None, "tp"),
            P("ep", None, "tp"),
            P("ep", "tp", None),
        ),
        out_specs=(P(("ep", "tp"), None), P(("ep", "tp"), None), P(("ep", "tp"), None)),
        check_vma=False,
    )
```

time: 187 us -> 93 us (0.50)
  Pallas kernels: 0 us -> 72.7 us
  waiting for transfers between devices: 49.9 us -> 0 us
  blocking collectives: 47.9 us -> 0 us
  matrix products: 30.7 us -> 0 us
  starting transfers between devices: 23.4 us -> 0 us
  between operations: 16 us -> 0.66 us
  local copies, waits for them, and re-layouts: 8.94 us -> 15.7 us
  other arithmetic: 8.78 us -> 3.39 us
    pallas_call x0 -> x1, Pallas kernels: none -> 72.7 us  [body(): pl.pallas_call(functools.partial(kernel, cfg), out_shape=(jax.ShapeDtypeS...]
    dot_general x18 -> x0, matrix products: 30.7 us -> none  [the longest x2 9.29 us: score_block(): jnp.einsum('shc,spc->shp', query_latent, latents, preferred_element_type=...]
    all_to_all x6 -> x0, waiting for transfers between devices: 26.3 us -> none  [the longest x1 8.57 us: body(): lax.all_to_all(summed, 'ep', split_axis=0, concat_axis=0, tiled=True)]
    all_gather x3 -> x0, blocking collectives: 25.2 us -> none  [the longest x1 10 us: body(): lax.all_gather(lax.all_to_all(sent, 'ep', split_axis=0, concat_axis=0, ti...]
    reduce_scatter x1 -> x0, waiting for transfers between devices: 23.6 us -> none  [body(): lax.psum_scatter(partial_out.astype(jnp.bfloat16), 'tp', scatter_dimensio...]
    all_to_all x6 -> x0, starting transfers between devices: 22.1 us -> none  [the longest x1 5.52 us: body(): lax.all_to_all(summed, 'ep', split_axis=0, concat_axis=0, tiled=True)]
    all_to_all x1 -> x0, blocking collectives: 14.1 us -> none  [body(): lax.all_to_all(sent, 'ep', split_axis=0, concat_axis=0, tiled=True)]
    unnamed x1 -> x0, blocking collectives: 8.63 us -> none
  transfers between devices with their start and end apart: 8 -> 0, of which waited for: 6 -> 0; matrix products, arithmetic and copies ran while one was open for 4% -> 0% of each run, Pallas kernels for 0% -> 0%
where the time goes in v1:
time: 93 us; the launch traced here: 92.4 us
  Pallas kernels  72.7 us (78%)
  local copies, waits for them, and re-layouts  15.7 us (17%)
  other arithmetic  3.39 us (4%)
    pallas_call x1, Pallas kernels, body(): pl.pallas_call(functools.partial(kernel, cfg), out_shape=(jax.ShapeDtypeS...  72.7 us
    unnamed x6, local copies, waits for them, and re-layouts  6.02 us
    another operation x4, local copies, waits for them, and re-layouts, body(): jnp.stack([attn_gain, post_attn_gain, ffn_gain, post_ffn_gain]).astype(F32)  2.77 us
    reshape x1, local copies, waits for them, and re-layouts, body(): w_value_up.reshape(C, LH * VD)  2.33 us

profile of v1, /device:TPU:0, one launch (start us, length us, event | category | flops | bytes accessed | tf_op | source)
XLA Modules:
  0.0 92.4 jit_solution(6131160360418086150)
XLA Ops:
  0.6 0.7 pad_convert_fusion
  1.3 1.3 %broadcast_in_dim.9 = f32[512]{0:T(512)} convert(bf16[512]{0:T(512)(128)(2,1)} %param.26) | non-fusion elementwise | flops 512 | bytes 3072 | tf_op jit(solution)/shard_map/broadcast_in_dim | solution.py:633
  2.6 0.7 stack.15
  3.3 0.7 stack.16
  3.9 0.7 stack.17
  4.6 0.7 stack.18
  5.3 0.7 maximum_convert_fusion.gains
  6.0 0.8 reshape.33
  6.8 0.8 reshape.31
  7.5 0.1 reshape.32
  7.6 0.0 copy-start
  7.6 0.1 fusion
  7.7 0.7 pad_maximum_fusion
  8.4 0.1 copy.24
  8.5 0.6 pad.19
  9.2 0.7 copy.25.routes
  9.9 1.5 %pad.16.tokens = bf16[16,2048]{1,0:T(8,128)(2,1)} pad(bf16[12,2048]{1,0:T(8,128)(2,1)} %param.21, bf16[]{:T(256)} %constant.3.clone.1), padding=0_4x0_0 | pad | bytes 114690 | tf_op jit(solution)/shard_map/jit(_pad)/pad | solution.py:537
  11.3 2.0 %copy.26.wkr_h = bf16[2048,64]{1,0:T(8,128)(2,1)} copy(bf16[2048,64]{0,1:T(8,128)(2,1)} %param.33) | data formatting | bytes 524288 | tf_op args[12]
  13.3 2.3 %copy_bitcast_fusion = (bf16[512,512]{1,0:T(8,128)(2,1)}, bf16[512,512]{1,0:T(8,128)(2,1)}) fusion(bf16[64,8,4,128]{3,2,1,0:T(4,128)(2,1)} %bitcast.15, bf16[64,8,4,128]{3,2,1,0:T(4,128)(2,1)} %bitcast.16), kind=kLoop, calls=%fused_computation | loop fusion | bytes 2097152 | tf_op jit(solution)/shard_map/reshape | solution.py:646
  15.6 0.0 copy-done
  15.6 72.7 %shard_map.220 = (bf16[12,2048]{1,0:T(8,128)(2,1)}, bf16[12,512]{1,0:T(8,128)(2,1)}, bf16[12,64]{1,0:T(8,128)(2,1)}) custom-call(s32[12]{0:T(128)} %lengths.1, bf16[16,2048]{1,0:T(8,128)(2,1)} %pad.16.tokens, f32[4,2048]{1,0:T(4,128)} %maximum_convert_fusion.gains, f32[1,512]{1,0:T(1,128)} %bitcast.19, f32[16,64]{1,0:T(8,128)} %get-tuple-element.6.cosine, ...), custom_call_target="tpu_custom_call" | custom-call | tf_op jit(solution)/shard_map/pallas_call | solution.py:561
  88.3 1.5 %copy.34 = bf16[12,2048]{1,0:T(8,128)(2,1)} copy(bf16[12,2048]{1,0:T(8,128)(2,1)} %get-tuple-element.13) | data formatting | bytes 98304
  89.8 1.3 %copy.35 = bf16[12,512]{1,0:T(8,128)(2,1)} copy(bf16[12,512]{1,0:T(8,128)(2,1)} %get-tuple-element.14) | data formatting | bytes 24576
  91.1 1.3 %copy.36 = bf16[12,64]{1,0:T(8,128)(2,1)} copy(bf16[12,64]{1,0:T(8,128)(2,1)} %get-tuple-element.15) | data formatting | bytes 3072
  (2 shorter events, 0.0 us)
Async XLA Ops:
  7.6 8.0 %copy-start = (s32[64,4]{0,1:T(4,128)}, s32[64,4]{0,1:T(4,128)S(1)}, u32[]{:S(2)}) copy-start(s32[64,4]{0,1:T(4,128)S(1)} %reshape.32) | copy-start | bytes 3076

commit v2 on v1

--- a/solution.py
+++ b/solution.py
@@ -2,6 +2,7 @@
 
 import jax
 import jax.numpy as jnp
+import numpy as np
 from jax import lax
 from jax.experimental import pallas as pl
 from jax.experimental.pallas import tpu as pltpu
@@ -50,13 +51,13 @@
     cfg,
     lengths,
     tokens,
-    gains,
+    attn_gain,
     latent_gain,
-    cosine,
-    sine,
-    routes,
+    post_attn_gain,
+    ffn_gain,
+    post_ffn_gain,
     routes_t,
-    logits,
+    logits_t,
     cache_h,
     rope_h,
     wq_h,
@@ -108,6 +109,11 @@
     ret,
     msend,
     mrecv,
+    ku3,
+    vu3,
+    wide,
+    sc,
+    pb,
     w_sem,
     c_sem,
     r_sem,
@@ -133,7 +139,7 @@
     e = lax.axis_index("ep")
     C = wku.shape[0]
     KD = wq.shape[1] // LH
-    RD = wkr.shape[1]
+    RD = wkr.shape[0]
     VD = wvu.shape[1] // LH
     LC = wl.shape[1]
     D = wq.shape[0]
@@ -150,8 +156,8 @@
             ("wqr", wqr_h, wqr),
             ("wl", wl_h, wl),
             ("wkr", wkr_h, wkr),
-            ("wku", wku_h, wku),
-            ("wvu", wvu_h, wvu),
+            ("wku", wku_h, ku3),
+            ("wvu", wvu_h, vu3),
             ("wo", wo_h, wo),
             ("wg", wg_h.at[0], wg),
             ("wu", wu_h.at[0], wu),
@@ -159,7 +165,7 @@
         ]
     ):
         loads[name] = pltpu.make_async_copy(src, dst, w_sem.at[i])
-    for name in ("wq", "wqr", "wl", "wkr", "wku"):
+    for name in ("wku", "wkr", "wq", "wqr", "wl"):
         loads[name].start()
 
     barrier = pltpu.get_barrier_semaphore()
@@ -178,8 +184,19 @@
     def rope_copy(b):
         return pltpu.make_async_copy(rope_h.at[b], rope.at[b], r_sem.at[b])
 
-    token_values = tokens[...].astype(F32)
-    xg[t] = rms_scale(token_values, gains[0:1, :]).astype(BF16)
+    def gain(ref):
+        return ref[...].astype(F32)[None, :]
+
+    def by_head_columns(source, target):
+        size = source.shape[2]
+        wide[...] = source[...].astype(F32).reshape(C * LH, size)
+        for h in range(LH):
+            target[:, h * size : (h + 1) * size] = wide[pl.ds(h, C, stride=LH), :].astype(BF16)
+
+    token_values = jnp.concatenate(
+        [tokens[...].astype(F32), jnp.zeros((RP - R, D), F32)], axis=0
+    )
+    xg[t] = rms_scale(token_values, gain(attn_gain)).astype(BF16)
     pl.semaphore_wait(barrier, T - 1 + EP - 1)
 
     def gather_tp(phase, buf):
@@ -220,12 +237,28 @@
     for b in range(R):
         cache_copy(b).start()
         rope_copy(b).start()
+    loads["wku"].wait()
+    by_head_columns(ku3, wku)
+    half = RD // 2
+    lane = lax.broadcasted_iota(jnp.int32, (RP, RD), 1)
+    row = lax.broadcasted_iota(jnp.int32, (RP, RD), 0)
+    freqs = jnp.zeros((RP, RD), F32)
+    for i in range(half):
+        hit = (lane == i) | (lane == i + half)
+        freqs = jnp.where(hit, np.float32(theta_base ** (-i / half)), freqs)
+    positions = jnp.zeros((RP, RD), jnp.int32)
+    for b in range(R):
+        positions = jnp.where(row == b, lengths[b], positions)
+    angles = positions.astype(F32) * freqs
+    cosine = jnp.cos(angles)
+    sine = jnp.sin(angles)
+    sine = jnp.where(lane < half, -sine, sine)
     loads["wkr"].wait()
-    key_raw = dot(xg[t], wkr[...]).astype(BF16).astype(F32)
-    new_rope = turn(key_raw, cosine[...], sine[...]).astype(BF16)
+    key_raw = dot_nt(xg[t], wkr[...]).astype(BF16).astype(F32)
+    new_rope = turn(key_raw, cosine, sine).astype(BF16)
     nrope[...] = new_rope.astype(F32)
     out_rope[...] = new_rope[:R]
-    for name in ("wq", "wqr", "wl", "wku"):
+    for name in ("wq", "wqr", "wl"):
         loads[name].wait()
     finish(copies)
 
@@ -257,7 +290,7 @@
     latent_raw = jnp.concatenate(
         [qrecv[s, :, base + LH * RD :] for s in range(T)], axis=1
     ).astype(F32)
-    new_latent = rms_scale(latent_raw, latent_gain[...]).astype(BF16)
+    new_latent = rms_scale(latent_raw, gain(latent_gain)).astype(BF16)
     out_latent[...] = new_latent[:R]
     nlat[...] = new_latent.astype(F32)
     stacked = jnp.concatenate(
@@ -268,8 +301,8 @@
         [
             turn(
                 qrecv[s, :, base + h * RD : base + (h + 1) * RD].astype(F32),
-                cosine[...],
-                sine[...],
+                cosine,
+                sine,
             ).astype(BF16)
             for s in range(T)
             for h in range(LH)
@@ -280,68 +313,67 @@
     if RP > R:
         hl[R:] = jnp.zeros((RP - R, H, C), BF16)
 
-    def attend(b, carry):
+    position = lax.broadcasted_iota(jnp.int32, (H, SPAN), 1)
+    for b in range(R):
         cache_copy(b).wait()
         rope_copy(b).wait()
-        q = qs[b]
-        qr = qt[b]
-        latents = cache[b]
-        fresh = nlat[pl.ds(b, 1), :]
-        fresh_rope = nrope[pl.ds(b, 1), :]
-        scores = (dot_nt(q, latents) + dot(qr, rope[b])) * scale
+        scores = (dot_nt(qs[b], cache[b]) + dot(qt[b], rope[b])) * scale
+        sc[b] = jnp.where(position < lengths[b], scores, -jnp.inf)
+    prob_own = []
+    for b in range(R):
         own = (
-            jnp.sum(q.astype(F32) * fresh, axis=1, keepdims=True)
-            + jnp.sum(qr.astype(F32) * fresh_rope, axis=1, keepdims=True)
+            jnp.sum(qs[b].astype(F32) * nlat[b : b + 1, :], axis=1, keepdims=True)
+            + jnp.sum(qt[b].astype(F32) * nrope[b : b + 1, :], axis=1, keepdims=True)
         ) * scale
-        valid = lax.broadcasted_iota(jnp.int32, (H, SPAN), 1) < lengths[b]
-        masked = jnp.where(valid, scores, -1e30)
+        masked = sc[b]
         highest = jnp.maximum(jnp.max(masked, axis=1, keepdims=True), own)
-        raised = jnp.where(valid, jnp.exp(masked - highest), 0.0)
+        raised = jnp.exp(masked - highest)
         raised_own = jnp.exp(own - highest)
-        total = jnp.sum(raised, axis=1, keepdims=True) + raised_own
-        inverse = 1.0 / total
-        probs = (raised * inverse).astype(BF16)
-        prob_own = (raised_own * inverse).astype(BF16).astype(F32)
-        hl[b] = (dot(probs, latents) + prob_own * fresh).astype(BF16)
-        return carry
-
-    lax.fori_loop(0, R, attend, 0)
+        inverse = 1.0 / (jnp.sum(raised, axis=1, keepdims=True) + raised_own)
+        pb[b] = (raised * inverse).astype(BF16)
+        prob_own.append((raised_own * inverse).astype(BF16).astype(F32))
+    for b in range(R):
+        hl[b] = (dot(pb[b], cache[b]) + prob_own[b] * nlat[b : b + 1, :]).astype(BF16)
 
     by_head = dot(to_head, hl[...].reshape(RP * H, C)).astype(BF16)
     hsend[...] = by_head.reshape(T, LH * RP, C)
     copies = scatter_tp(2, hsend, hrecv)
     loads["wvu"].wait()
+    by_head_columns(vu3, wvu)
     loads["wo"].wait()
 
+    N = routes_t.shape[1]
     slot_shift = CP.bit_length() - 1
-    s_lane = lax.broadcasted_iota(jnp.int32, (G, S), 1)
-    e_lane = s_lane >> slot_shift
-    c_lane = (s_lane & (CP - 1)).astype(F32)
-    s_sub = lax.broadcasted_iota(jnp.int32, (S, G), 0)
+    s_sub = lax.broadcasted_iota(jnp.int32, (S, N), 0)
     e_sub = s_sub >> slot_shift
     c_sub = (s_sub & (CP - 1)).astype(F32)
-    gi = lax.broadcasted_iota(jnp.int32, (G, G), 0)
-    gj = lax.broadcasted_iota(jnp.int32, (G, G), 1)
-    lower = (gj < gi).astype(F32).astype(BF16)
+    gi = lax.broadcasted_iota(jnp.int32, (N, N), 0)
+    gj = lax.broadcasted_iota(jnp.int32, (N, N), 1)
     upper = (gi < gj).astype(F32).astype(BF16)
-    K = routes.shape[1]
-    lg = logits[...]
-    lg = jnp.exp(lg - jnp.max(lg, axis=1, keepdims=True))
-    weights = lg / jnp.sum(lg, axis=1, keepdims=True)
-    count = jnp.zeros((G, S), F32)
-    weighted = jnp.zeros((G, S), F32)
-    count_t = jnp.zeros((S, G), F32)
-    for k in range(K):
-        hit = routes[:, k : k + 1] == e_lane
+    pi = lax.broadcasted_iota(jnp.int32, (G, N), 0)
+    pj = lax.broadcasted_iota(jnp.int32, (G, N), 1)
+    spread = jnp.zeros((G, N), F32)
+    for s in range(T):
+        inside = (pj >= s * R) & (pj < (s + 1) * R)
+        spread = jnp.where(inside & (pi == pj + s * (RP - R)), 1.0, spread)
+    spread = spread.astype(BF16)
+    lg = logits_t[...]
+    lg = jnp.exp(lg - jnp.max(lg, axis=0, keepdims=True))
+    weights = lg / jnp.sum(lg, axis=0, keepdims=True)
+    count = jnp.zeros((S, N), F32)
+    weighted = jnp.zeros((S, N), F32)
+    for k in range(routes_t.shape[0]):
+        hit = routes_t[k : k + 1, :] == e_sub
         count = jnp.where(hit, 1.0, count)
-        weighted = jnp.where(hit, weights[:, k : k + 1], weighted)
-        count_t = jnp.where(routes_t[k : k + 1, :] == e_sub, 1.0, count_t)
-    rank = dot(lower, count.astype(BF16))
-    rank_t = dot(count_t.astype(BF16), upper)
-    combine = jnp.where(rank == c_lane, weighted, 0.0)
-    combine_hi = combine.astype(BF16)
-    combine_lo = (combine - combine_hi.astype(F32)).astype(BF16)
-    dispatch = jnp.where(rank_t == c_sub, count_t, 0.0).astype(BF16)
+        weighted = jnp.where(hit, weights[k : k + 1, :], weighted)
+    rank = dot(count.astype(BF16), upper)
+    taken = rank == c_sub
+    weighted = jnp.where(taken, weighted, 0.0)
+    weighted_hi = weighted.astype(BF16)
+    weighted_lo = (weighted - weighted_hi.astype(F32)).astype(BF16)
+    combine_hi = dot_nt(spread, weighted_hi).astype(BF16)
+    combine_lo = dot_nt(spread, weighted_lo).astype(BF16)
+    dispatch = dot_nt(jnp.where(taken, count, 0.0).astype(BF16), spread).astype(BF16)
 
     finish(copies)
     values = []
@@ -357,8 +389,8 @@
     for s in range(1, T):
         attn = attn + arecv[s].astype(F32)
     attn = attn.astype(BF16).astype(F32)
-    mixed = (token_values + rms_scale(attn, gains[1:2, :])).astype(BF16).astype(F32)
-    fg[t] = rms_scale(mixed, gains[2:3, :]).astype(BF16)
+    mixed = (token_values + rms_scale(attn, gain(post_attn_gain))).astype(BF16).astype(F32)
+    fg[t] = rms_scale(mixed, gain(ffn_gain)).astype(BF16)
     finish(gather_tp(4, fg))
 
     mine = fg[:, :, pl.ds(pl.multiple_of(t * Q, Q), Q)].reshape(G, Q)
@@ -479,7 +511,7 @@
     msend[...] = moe_part.astype(BF16).reshape(T, RP, Q)
     finish(scatter_tp(5, msend, mrecv))
     moe = jnp.concatenate([mrecv[s] for s in range(T)], axis=1).astype(F32)
-    out_result[...] = (mixed + rms_scale(moe, gains[3:4, :])).astype(BF16)[:R]
+    out_result[...] = (mixed + rms_scale(moe, gain(post_ffn_gain))).astype(BF16)[:R]
 
     for c in sent[1:] + to_sib + [c for row in across for c in row] + back:
         c.wait_send()
@@ -488,6 +520,12 @@
     for row in reduced:
         for c in row[1:]:
             c.wait_send()
+
+
+def hand_over(result, latent, rope, out_result, out_latent, out_rope):
+    out_result[...] = result[...]
+    out_latent[...] = latent[...]
+    out_rope[...] = rope[...]
 
 
 def body(
@@ -534,20 +572,6 @@
     LC = w_latent.shape[1]
     SPAN = cache_latent.shape[1]
 
-    padded = jnp.pad(tokens, ((0, RP - R), (0, 0)))
-    gains = jnp.stack([attn_gain, post_attn_gain, ffn_gain, post_ffn_gain]).astype(F32)
-    half = RD // 2
-    freqs = theta_base ** (-jnp.arange(half, dtype=F32) / half)
-    angles = jnp.pad(lengths, (0, RP - R)).astype(F32)[:, None] * freqs
-    cosine = jnp.cos(angles)
-    sine = jnp.sin(angles)
-    cosine = jnp.concatenate([cosine, cosine], axis=1)
-    sine = jnp.concatenate([-sine, sine], axis=1)
-    rt = jnp.pad(routes.reshape(T, R, K), ((0, 0), (0, RP - R), (0, 0)), constant_values=-1)
-    rt = rt.reshape(T * RP, K)
-    lg = jnp.pad(route_logits.reshape(T, R, K), ((0, 0), (0, RP - R), (0, 0)))
-    lg = lg.reshape(T * RP, K)
-
     vm = pl.BlockSpec(memory_space=pltpu.VMEM)
     hbm = pl.BlockSpec(memory_space=pl.ANY)
     dma = pltpu.SemaphoreType.DMA
@@ -558,7 +582,7 @@
         return pltpu.VMEM(shape, dtype)
 
     cfg = (T, EP, R, RP, LH, CP, scale)
-    return pl.pallas_call(
+    outs = pl.pallas_call(
         functools.partial(kernel, cfg),
         out_shape=(
             jax.ShapeDtypeStruct((R, D), BF16),
@@ -573,7 +597,7 @@
             v(D, LH * KD),
             v(D, LH * RD),
             v(D, LC),
-            v(D, RD),
+            v(RD, D),
             v(C, LH * KD),
             v(C, LH * VD),
             v(LH * VD, D),
@@ -604,6 +628,11 @@
             v(EP, CP, Q),
             v(T, RP, Q),
             v(T, RP, Q),
+            v(C, LH, KD),
+            v(C, LH, VD),
+            v(C * LH, KD, dtype=F32),
+            v(R, H, SPAN, dtype=F32),
+            v(R, H, SPAN),
             dma((10,)),
             dma((R,)),
             dma((R,)),
@@ -628,27 +657,33 @@
         ),
     )(
         lengths,
-        padded,
-        gains,
-        latent_gain.astype(F32)[None, :],
-        cosine,
-        sine,
-        rt,
-        rt.T,
-        lg,
+        tokens,
+        attn_gain,
+        latent_gain,
+        post_attn_gain,
+        ffn_gain,
+        post_ffn_gain,
+        routes.T,
+        route_logits.T,
         cache_latent,
         cache_rope,
         w_query,
         w_query_rot,
         w_latent,
-        w_key_rot,
-        w_key_up.reshape(C, LH * KD),
-        w_value_up.reshape(C, LH * VD),
+        w_key_rot.T,
+        w_key_up,
+        w_value_up,
         w_out,
         w_gate,
         w_up,
         w_down,
     )
+    return pl.pallas_call(
+        hand_over,
+        out_shape=tuple(jax.ShapeDtypeStruct(o.shape, o.dtype) for o in outs),
+        in_specs=[vm] * 3,
+        out_specs=(vm, vm, vm),
+    )(*outs)
 
 
 def solution(mesh):

time: 93 us -> 76.2 us (0.82)
  local copies, waits for them, and re-layouts: 15.7 us -> 0 us
  other arithmetic: 3.39 us -> 0 us
  Pallas kernels: 72.7 us -> 75.4 us
    unnamed x6 -> x0, local copies, waits for them, and re-layouts: 6.02 us -> none
    reshape x6 -> x0, local copies, waits for them, and re-layouts: 4.76 us -> none  [the longest x1 2.33 us: body(): w_value_up.reshape(C, LH * VD)]
    another operation x4 -> x0, local copies, waits for them, and re-layouts: 2.77 us -> none  [body(): jnp.stack([attn_gain, post_attn_gain, ffn_gain, post_ffn_gain]).astype(F32)]
    pad x3 -> x0, local copies, waits for them, and re-layouts: 2.11 us -> none  [the longest x1 1.48 us: body(): padded = jnp.pad(tokens, ((0, RP - R), (0, 0)))]
    pallas_call x0 -> x1, Pallas kernels: none -> 1.5 us  [body(): pl.pallas_call(hand_over, out_shape=tuple((jax.ShapeDtypeStruct(o.shape,...]
    convert_element_type x2 -> x0, other arithmetic: 1.32 us -> none  [the longest x1 0.66 us: body(): angles = jnp.pad(lengths, (0, RP - R)).astype(F32)[:, None] * freqs]
    broadcast_in_dim x1 -> x0, other arithmetic: 1.26 us -> none  [body(): latent_gain.astype(F32)[None, :]]
    pallas_call x1, Pallas kernels: 72.7 us -> 73.9 us  [body(): pl.pallas_call(functools.partial(kernel, cfg), out_shape=(jax.ShapeDtypeS...]
where the time goes in v2:
time: 76.2 us; the launch traced here: 76 us
  Pallas kernels  75.4 us (99%)
    pallas_call x1, Pallas kernels, body(): pl.pallas_call(functools.partial(kernel, cfg), out_shape=(jax.ShapeDtypeS...  73.9 us

profile of v2, /device:TPU:0, one launch (start us, length us, event | category | flops | bytes accessed | tf_op | source)
XLA Modules:
  0.0 76.0 jit_solution(3909874431465672118)
XLA Ops:
  0.6 73.9 %shard_map.220 = (bf16[12,2048]{1,0:T(8,128)(2,1)}, bf16[12,512]{1,0:T(8,128)(2,1)}, bf16[12,64]{1,0:T(8,128)(2,1)}) custom-call(s32[12]{0:T(128)} %lengths.1, bf16[12,2048]{1,0:T(8,128)(2,1)} %tokens.1, bf16[2048]{0:T(1024)(128)(2,1)} %attn_gain.1, bf16[512]{0:T(512)(128)(2,1)} %latent_gain.1, bf16[2048]{0:T(1024)(128)(2,1)} %post_attn_gain.1, ...), custom_call_target="tpu_custom_call" | custom-call | tf_op jit(solution)/shard_map/pallas_call | solution.py:585
  74.5 1.5 %shard_map.221 = (bf16[12,2048]{1,0:T(8,128)(2,1)}, bf16[12,512]{1,0:T(8,128)(2,1)}, bf16[12,64]{1,0:T(8,128)(2,1)}) custom-call(bf16[12,2048]{1,0:T(8,128)(2,1)} %get-tuple-element.6.result, bf16[12,512]{1,0:T(8,128)(2,1)} %get-tuple-element.7.latent, bf16[12,64]{1,0:T(8,128)(2,1)} %get-tuple-element.8.rope), custom_call_target="tpu_custom_call" | custom-call | tf_op jit(solution)/shard_map/pallas_call | solution.py:681
